TPU v7x, 32 devices: a whole 2x2x4 slice. The times are simulated.
32 devices in a mesh: rep: 2 (over x), fs: 8 (over z, y), tp: 2 (over core).
Axes of the slice: x: 2, y: 2, z: 4, core: 2. Of those that a mesh axis runs over, the one named last changes fastest.
Arguments:
- tokens: bfloat16 [8192, 2048], P(('rep', 'fs')), may hold values from -6 to 6
- mix_gain: bfloat16 [2048], replicated, may hold values from 0.099609375 to 1.8984375
- value_weight: bfloat16 [2048, 1536], P('fs', 'tp'), may hold values from -0.125 to 0.125
- outer_gate_weight: bfloat16 [2048, 1536], P('fs', 'tp'), may hold values from -0.125 to 0.125
- inner_gate_weight: bfloat16 [2048, 1536], P('fs', 'tp'), may hold values from -0.125 to 0.125
- conv_taps: bfloat16 [3, 1536], P(None, 'tp'), may hold values from -3 to 3
- mix_out_weight: bfloat16 [1536, 2048], P('tp', 'fs'), may hold values from -0.15625 to 0.15625
- ffn_gain: bfloat16 [2048], replicated, may hold values from 0.099609375 to 1.8984375
- gate_weight: bfloat16 [2048, 4096], P('fs', 'tp'), may hold values from -0.125 to 0.125
- up_weight: bfloat16 [2048, 4096], P('fs', 'tp'), may hold values from -0.125 to 0.125
- down_weight: bfloat16 [4096, 2048], P('tp', 'fs'), may hold values from -0.09375 to 0.09375
Outputs:
- layer_out: bfloat16 [8192, 2048], P(('rep', 'fs'))
All inputs are finite; a program needn't handle non-finite values.
Results may differ from a plain program's by a relative error of at most 0.02.
Values may be sent and summed in bfloat16 or wider, within the bound.
A program may use at most 128 MiB of HBM per device.

v0:
```python
import jax
import jax.numpy as jnp
from jax import lax
from jax.sharding import PartitionSpec as P

SEQ_GRP = 2
EPS = 1e-05


def rms_norm(values, gain):
    floats = values.astype(jnp.float32)
    scaled = floats * lax.rsqrt(jnp.mean(floats * floats, axis=-1, keepdims=True) + EPS)
    return (scaled * gain.astype(jnp.float32)).astype(jnp.bfloat16)


def short_conv(value_proj, outer_proj, inner_proj, conv_taps, seq_len):
    mixed_in = inner_proj.astype(jnp.float32) * value_proj.astype(jnp.float32)
    count_rows = mixed_in.shape[0]
    position = (jnp.arange(count_rows, dtype=jnp.int32) % seq_len)[:, None]
    zero_row = jnp.zeros((1, mixed_in.shape[1]), jnp.float32)
    back_one = jnp.where(position >= 1, jnp.concatenate([zero_row, mixed_in[:-1]], axis=0), 0.0)
    back_two = jnp.where(
        position >= 2, jnp.concatenate([zero_row, zero_row, mixed_in[:-2]], axis=0), 0.0
    )
    taps = conv_taps.astype(jnp.float32)
    convolved = taps[0] * back_two + taps[1] * back_one + taps[2] * mixed_in
    return (outer_proj.astype(jnp.float32) * convolved).astype(jnp.bfloat16)


def local(
    tokens,
    mix_gain,
    value_weight,
    outer_gate_weight,
    inner_gate_weight,
    conv_taps,
    mix_out_weight,
    ffn_gain,
    gate_weight,
    up_weight,
    down_weight,
):
    row_count = tokens.shape[0]
    share = row_count // lax.axis_size("tp")
    seq_len = row_count // SEQ_GRP
    own_rows = lax.dynamic_slice_in_dim(tokens, lax.axis_index("tp") * share, share, 0).astype(
        jnp.float32
    )
    normed = rms_norm(tokens, mix_gain)
    value_full, outer_full, inner_full, mix_out_full, gate_full, up_full, down_full = (
        lax.all_gather(value_weight, "fs", axis=0, tiled=True),
        lax.all_gather(outer_gate_weight, "fs", axis=0, tiled=True),
        lax.all_gather(inner_gate_weight, "fs", axis=0, tiled=True),
        lax.all_gather(mix_out_weight, "fs", axis=1, tiled=True),
        lax.all_gather(gate_weight, "fs", axis=0, tiled=True),
        lax.all_gather(up_weight, "fs", axis=0, tiled=True),
        lax.all_gather(down_weight, "fs", axis=1, tiled=True),
    )
    value_proj = jnp.dot(normed, value_full, preferred_element_type=jnp.float32).astype(
        jnp.bfloat16
    )
    outer_proj = jnp.dot(normed, outer_full, preferred_element_type=jnp.float32).astype(
        jnp.bfloat16
    )
    inner_proj = jnp.dot(normed, inner_full, preferred_element_type=jnp.float32).astype(
        jnp.bfloat16
    )
    mixed = short_conv(value_proj, outer_proj, inner_proj, conv_taps, seq_len)
    picked = mixed
    mix_total = lax.psum_scatter(
        jnp.dot(picked, mix_out_full, preferred_element_type=jnp.float32).astype(jnp.bfloat16),
        "tp",
        scatter_dimension=0,
        tiled=True,
    ).astype(jnp.float32)
    after_mix = (own_rows + mix_total).astype(jnp.bfloat16)
    normed_two = rms_norm(after_mix, ffn_gain)
    block_rows = lax.all_gather(normed_two, "tp", axis=0, tiled=True)
    gate_proj = jnp.dot(block_rows, gate_full, preferred_element_type=jnp.float32)
    up_proj = jnp.dot(block_rows, up_full, preferred_element_type=jnp.float32)
    hidden = (jax.nn.silu(gate_proj) * up_proj).astype(jnp.bfloat16)
    picked = hidden
    ffn_total = lax.psum_scatter(
        jnp.dot(picked, down_full, preferred_element_type=jnp.float32).astype(jnp.bfloat16),
        "tp",
        scatter_dimension=0,
        tiled=True,
    ).astype(jnp.float32)
    finished = (after_mix.astype(jnp.float32) + ffn_total).astype(jnp.bfloat16)
    return lax.all_gather(finished, "tp", axis=0, tiled=True)


def solution(mesh):
    placed = (
        P(("rep", "fs"), None),
        P(),
        P("fs", "tp"),
        P("fs", "tp"),
        P("fs", "tp"),
        P(None, "tp"),
        P("tp", "fs"),
        P(),
        P("fs", "tp"),
        P("fs", "tp"),
        P("tp", "fs"),
    )
    return jax.shard_map(
        local, mesh=mesh, in_specs=placed, out_specs=P(("rep", "fs"), None), check_vma=False
    )
```

profile of v0, /device:TPU:0, one launch (start us, length us, event | category | flops | bytes accessed | tf_op | source)
XLA Modules:
  0.0 718.0 jit_solution(16249208888733937228)
XLA Ops:
  6.5 0.0 all-gather.14.cloned.1.call-start
  6.5 0.7 all-gather.14.cloned.1.call-update
  7.3 0.0 all-gather.12.cloned.1.call-start
  7.3 0.7 all-gather.12.cloned.1.call-update
  8.0 0.0 all-gather.10.cloned.1.call-start
  8.1 0.7 all-gather.10.cloned.1.call-update
  8.7 0.0 all-gather.16.cloned.1.call-start
  8.8 0.5 all-gather.16.cloned.1.call-update
  9.3 0.0 reduce-scatter.3.cloned.1.call-start
  9.4 0.7 convert_element_type.69
  10.1 0.7 convert_element_type.73
  10.8 2.1 fusion
  12.9 59.4 %all-gather.14.cloned.1.call-done = bf16[2048,768]{1,0:T(8,128)(2,1)} async-done(((bf16[256,768]{1,0:T(8,128)(2,1)}), bf16[2048,768]{1,0:T(8,128)(2,1)}) %all-gather.14.cloned.1.call-update) | async-done | bytes 3145744 | tf_op jit(solution)/shard_map/all_gather | solution.py:51
  72.3 0.0 copy-done
  72.3 3.7 convolution_convert_fusion.2
  76.0 57.2 %all-gather.12.cloned.1.call-done = bf16[2048,768]{1,0:T(8,128)(2,1)} async-done(((bf16[256,768]{1,0:T(8,128)(2,1)}), bf16[2048,768]{1,0:T(8,128)(2,1)}) %all-gather.12.cloned.1.call-update) | async-done | bytes 3145744 | tf_op jit(solution)/shard_map/all_gather | solution.py:53
  133.2 4.9 convert_multiply_fusion.4
  138.1 56.0 %all-gather.10.cloned.1.call-done = bf16[2048,768]{1,0:T(8,128)(2,1)} async-done(((bf16[256,768]{1,0:T(8,128)(2,1)}), bf16[2048,768]{1,0:T(8,128)(2,1)}) %all-gather.10.cloned.1.call-update) | async-done | bytes 3145744 | tf_op jit(solution)/shard_map/all_gather | solution.py:52
  194.1 63.2 %all-gather.16.cloned.1.call-done = bf16[768,2048]{1,0:T(8,128)(2,1)} async-done(((bf16[768,256]{1,0:T(8,128)(2,1)}), bf16[768,2048]{1,0:T(8,128)(2,1)}) %all-gather.16.cloned.1.call-update) | async-done | bytes 3145744 | tf_op jit(solution)/shard_map/all_gather | solution.py:54
  257.3 9.8 %convolution_convert_fusion.1 = bf16[512,2048]{1,0:T(8,128)(2,1)} fusion(bf16[768,2048]{1,0:T(8,128)(2,1)} %all-gather.16.cloned.1.call-done, f32[512,768]{1,0:T(8,128)} %convert_multiply_fusion.4, f32[511,768]{1,0:T(8,128)} %bitcast.20, f32[510,768]{1,0:T(8,128)} %bitcast.21, bf16[2048,768]{1,0:T(8,128)(2,1)} %all-gather.10.cloned.1.call-done, ...), kind=kOutput, calls=%fused_computation.10 | convolution fusion | flops 3230793728 | bytes 15215616 | tf_op jit(solution)/shard_map/dot_general | solution.py:71
  267.2 0.0 reduce-scatter.3.cloned.1.call-update
  267.2 0.0 all-gather.18.cloned.1.call-start
  267.2 0.6 copy-done.1
  267.8 7.4 %reduce-scatter.3.cloned.1.call-done = bf16[256,2048]{1,0:T(8,128)(2,1)} async-done(((bf16[512,2048]{1,0:T(8,128)(2,1)}), bf16[256,2048]{1,0:T(8,128)(2,1)}) %reduce-scatter.3.cloned.1.call-update) | async-done | bytes 1048592 | tf_op jit(solution)/shard_map/reduce_scatter | solution.py:70
  275.3 1.7 fusion.3
  277.0 1.3 fusion.5
  278.3 0.0 all-gather.18.cloned.1.call-update
  278.3 0.0 all-gather.20.cloned.1.call-start
  278.4 0.7 all-gather.20.cloned.1.call-update
  279.1 0.0 all-gather.22.cloned.1.call-start
  279.1 0.7 all-gather.22.cloned.1.call-update
  279.8 0.0 all-gather.24.cloned.1.call-start
  279.9 0.7 all-gather.24.cloned.1.call-update
  280.6 0.2 reduce-scatter.5.cloned.1.call-start
  280.8 9.6 %all-gather.18.cloned.1.call-done = bf16[512,2048]{1,0:T(8,128)(2,1)} async-done(((bf16[256,2048]{1,0:T(8,128)(2,1)}), bf16[512,2048]{1,0:T(8,128)(2,1)}) %all-gather.18.cloned.1.call-update) | async-done | bytes 2097168 | tf_op jit(solution)/shard_map/all_gather | solution.py:78
  290.4 127.8 %all-gather.20.cloned.1.call-done = bf16[2048,2048]{1,0:T(8,128)(2,1)} async-done(((bf16[256,2048]{1,0:T(8,128)(2,1)}), bf16[2048,2048]{1,0:T(8,128)(2,1)}) %all-gather.20.cloned.1.call-update) | async-done | bytes 8388624 | tf_op jit(solution)/shard_map/all_gather | solution.py:55
  418.2 10.5 %fusion.17 = f32[512,2048]{1,0:T(8,128)} fusion(bf16[512,2048]{1,0:T(8,128)(2,1)} %all-gather.18.cloned.1.call-done, bf16[2048,2048]{1,0:T(8,128)(2,1)} %all-gather.20.cloned.1.call-done), kind=kOutput, calls=%fused_computation.34 | convolution fusion | flops 4294967296 | bytes 14680064 | tf_op jit(solution)/shard_map/dot_general | solution.py:79
  428.6 114.3 %all-gather.22.cloned.1.call-done = bf16[2048,2048]{1,0:T(8,128)(2,1)} async-done(((bf16[256,2048]{1,0:T(8,128)(2,1)}), bf16[2048,2048]{1,0:T(8,128)(2,1)}) %all-gather.22.cloned.1.call-update) | async-done | bytes 8388624 | tf_op jit(solution)/shard_map/all_gather | solution.py:56
  543.0 125.2 %all-gather.24.cloned.1.call-done = bf16[2048,2048]{1,0:T(8,128)(2,1)} async-done(((bf16[2048,256]{1,0:T(8,128)(2,1)}), bf16[2048,2048]{1,0:T(8,128)(2,1)}) %all-gather.24.cloned.1.call-update) | async-done | bytes 8388624 | tf_op jit(solution)/shard_map/all_gather | solution.py:57
  668.2 0.0 copy-done.2
  668.2 17.4 %convolution_convert_fusion = bf16[512,2048]{1,0:T(8,128)(2,1)} fusion(bf16[2048,2048]{1,0:T(8,128)(2,1)} %all-gather.24.cloned.1.call-done, f32[512,2048]{1,0:T(8,128)} %fusion.17, bf16[512,2048]{1,0:T(8,128)(2,1)S(1)} %copy-done.2, bf16[2048,2048]{1,0:T(8,128)(2,1)} %all-gather.22.cloned.1.call-done), kind=kOutput, calls=%fused_computation.9 | convolution fusion | flops 8597274624 | bytes 25165824 | tf_op jit(solution)/shard_map/dot_general | solution.py:84
  685.6 0.0 reduce-scatter.5.cloned.1.call-update
  685.6 0.0 all-gather.26.cloned.1.call-start
  685.7 8.0 %reduce-scatter.5.cloned.1.call-done = bf16[256,2048]{1,0:T(8,128)(2,1)} async-done(((bf16[512,2048]{1,0:T(8,128)(2,1)}), bf16[256,2048]{1,0:T(8,128)(2,1)}) %reduce-scatter.5.cloned.1.call-update) | async-done | bytes 1048592 | tf_op jit(solution)/shard_map/reduce_scatter | solution.py:83
  693.7 2.6 fusion.6
  696.3 0.0 all-gather.26.cloned.1.call-update
  696.3 12.0 %all-gather.26.cloned.1.call-done = bf16[512,2048]{1,0:T(8,128)(2,1)} async-done(((bf16[256,2048]{1,0:T(8,128)(2,1)}), bf16[512,2048]{1,0:T(8,128)(2,1)}) %all-gather.26.cloned.1.call-update) | async-done | bytes 2097168 | tf_op jit(solution)/shard_map/all_gather | solution.py:90
  708.3 3.2 copy.13
  (8 shorter events, 0.1 us)
Async XLA Ops:
  6.5 65.8 %copy-start = (bf16[512,2048]{1,0:T(8,128)(2,1)S(1)}, bf16[512,2048]{1,0:T(8,128)(2,1)}, u32[]{:S(2)}) copy-start(bf16[512,2048]{1,0:T(8,128)(2,1)} %param.11) | copy-start | bytes 6291460
  6.5 65.8 %all-gather.14.cloned.1.call-start = ((), (), s32[]{:S(2)}) async-start(), calls=%async_computation.4 | async-start | bytes 3538944 | tf_op jit(solution)/shard_map/all_gather | solution.py:51
  7.3 125.9 %all-gather.12.cloned.1.call-start = ((), (), s32[]{:S(2)}) async-start(), calls=%async_computation.3 | async-start | bytes 3538944 | tf_op jit(solution)/shard_map/all_gather | solution.py:53
  8.0 186.1 %all-gather.10.cloned.1.call-start = ((), (), s32[]{:S(2)}) async-start(), calls=%async_computation.2 | async-start | bytes 3538944 | tf_op jit(solution)/shard_map/all_gather | solution.py:52
  8.7 248.6 %all-gather.16.cloned.1.call-start = ((), (), s32[]{:S(2)}) async-start(), calls=%async_computation.5 | async-start | bytes 3538944 | tf_op jit(solution)/shard_map/all_gather | solution.py:54
  9.3 266.0 %reduce-scatter.3.cloned.1.call-start = ((), (), s32[]{:S(2)}) async-start(), calls=%async_computation.6 | async-start | bytes 3145728 | tf_op jit(solution)/shard_map/reduce_scatter | solution.py:70
  267.2 0.7 copy-start.1
  267.2 23.2 %all-gather.18.cloned.1.call-start = ((), (), s32[]{:S(2)}) async-start(), calls=%async_computation.7 | async-start | bytes 3145728 | tf_op jit(solution)/shard_map/all_gather | solution.py:78
  278.3 139.8 %all-gather.20.cloned.1.call-start = ((), (), s32[]{:S(2)}) async-start(), calls=%async_computation.8 | async-start | bytes 9437184 | tf_op jit(solution)/shard_map/all_gather | solution.py:55
  279.1 263.9 %all-gather.22.cloned.1.call-start = ((), (), s32[]{:S(2)}) async-start(), calls=%async_computation.9 | async-start | bytes 9437184 | tf_op jit(solution)/shard_map/all_gather | solution.py:56
  279.8 388.3 %all-gather.24.cloned.1.call-start = ((), (), s32[]{:S(2)}) async-start(), calls=%async_computation.10 | async-start | bytes 9437184 | tf_op jit(solution)/shard_map/all_gather | solution.py:57
  280.6 413.1 %reduce-scatter.5.cloned.1.call-start = ((), (), s32[]{:S(2)}) async-start(), calls=%async_computation.11 | async-start | bytes 3145728 | tf_op jit(solution)/shard_map/reduce_scatter | solution.py:83
  290.4 377.8 %copy-start.2 = (bf16[512,2048]{1,0:T(8,128)(2,1)S(1)}, bf16[512,2048]{1,0:T(8,128)(2,1)}, u32[]{:S(2)}) copy-start(bf16[512,2048]{1,0:T(8,128)(2,1)} %all-gather.18.cloned.1.call-done) | copy-start | bytes 6291460
  685.6 22.7 %all-gather.26.cloned.1.call-start = ((), (), s32[]{:S(2)}) async-start(), calls=%async_computation.12 | async-start | bytes 3145728 | tf_op jit(solution)/shard_map/all_gather | solution.py:90
Sparse Core Ops, SparseCore 0:
  9.5 62.7 all-gather.13
  74.5 58.6 all-gather.11
  135.4 58.6 all-gather.9
  196.0 61.3 all-gather.15
  267.3 7.9 reduce-scatter.2
  278.5 11.8 all-gather.17
  292.5 125.6 all-gather.19
  420.3 122.6 all-gather.21
  545.0 123.1 all-gather.23
  685.7 7.9 reduce-scatter.4
  696.4 11.8 all-gather.25
where the time goes:
time: 718 us
  waiting for transfers between devices  645 us (90%)
  matrix products  46.3 us (6%)
  between operations  13.3 us (2%)
  other arithmetic  9.09 us (1%)
    all_gather x1, waiting for transfers between devices, local(): lax.all_gather(gate_weight, 'fs', axis=0, tiled=True)  128 us
    all_gather x1, waiting for transfers between devices, local(): lax.all_gather(down_weight, 'fs', axis=1, tiled=True)  125 us
    all_gather x1, waiting for transfers between devices, local(): lax.all_gather(up_weight, 'fs', axis=0, tiled=True)  114 us
    all_gather x1, waiting for transfers between devices, local(): lax.all_gather(mix_out_weight, 'fs', axis=1, tiled=True)  63.2 us
    all_gather x1, waiting for transfers between devices, local(): lax.all_gather(value_weight, 'fs', axis=0, tiled=True)  59.4 us
    all_gather x1, waiting for transfers between devices, local(): lax.all_gather(inner_gate_weight, 'fs', axis=0, tiled=True)  57.2 us
    all_gather x1, waiting for transfers between devices, local(): lax.all_gather(outer_gate_weight, 'fs', axis=0, tiled=True)  56 us
    dot_general x1, matrix products, local(): jnp.dot(picked, down_full, preferred_element_type=jnp.float32)  17.4 us
  transfers between devices with their start and end apart: 11, of which 11 were waited for; matrix products, arithmetic and copies ran while one was open for 3% of the time, Pallas kernels for 0%

commit v1 on v0

--- a/solution.py
+++ b/solution.py
@@ -5,6 +5,23 @@
 
 SEQ_GRP = 2
 EPS = 1e-05
+
+
+def in_order(blocks, dim):
+    shape = list(blocks.shape[1:])
+    shape[dim] *= blocks.shape[0]
+    return jnp.moveaxis(blocks, 0, dim).reshape(shape)
+
+
+def gather_around(x, axis, dim):
+    size = lax.axis_size(axis)
+    right = [(i, (i + 1) % size) for i in range(size)]
+    parts = [x]
+    while len(parts) < size:
+        parts.append(lax.ppermute(parts[-1], axis, right))
+    index = lax.axis_index(axis)
+    parts = jnp.stack(parts)[(index - jnp.arange(size)) % size]
+    return in_order(parts, dim)
 
 
 def rms_norm(values, gain):
@@ -51,7 +68,7 @@
         lax.all_gather(value_weight, "fs", axis=0, tiled=True),
         lax.all_gather(outer_gate_weight, "fs", axis=0, tiled=True),
         lax.all_gather(inner_gate_weight, "fs", axis=0, tiled=True),
-        lax.all_gather(mix_out_weight, "fs", axis=1, tiled=True),
+        gather_around(mix_out_weight, "fs", 1),
         lax.all_gather(gate_weight, "fs", axis=0, tiled=True),
         lax.all_gather(up_weight, "fs", axis=0, tiled=True),
         lax.all_gather(down_weight, "fs", axis=1, tiled=True),

time: 718 us -> 689 us (0.960)
  waiting for transfers between devices: 645 us -> 601 us
  local copies, waits for them, and re-layouts: 3.81 us -> 14.9 us
    ppermute x0 -> x7, waiting for transfers between devices: none -> 114 us  [gather_around(): parts.append(lax.ppermute(parts[-1], axis, right))]
    all_gather x1 -> x0, waiting for transfers between devices: 63.2 us -> none  [local(): lax.all_gather(mix_out_weight, 'fs', axis=1, tiled=True)]
    all_gather x1, waiting for transfers between devices: 59.4 us -> 0.01 us  [local(): lax.all_gather(value_weight, 'fs', axis=0, tiled=True)]
    all_gather x1, waiting for transfers between devices: 57.2 us -> 22.4 us  [local(): lax.all_gather(inner_gate_weight, 'fs', axis=0, tiled=True)]
  transfers between devices with their start and end apart: 11 -> 17, of which waited for: 11 -> 16; matrix products, arithmetic and copies ran while one was open for 3% -> 5% of each run, Pallas kernels for 0% -> 0%
where the time goes in v1:
time: 689 us
  waiting for transfers between devices  601 us (87%)
  matrix products  47.3 us (7%)
  local copies, waits for them, and re-layouts  14.9 us (2%)
  between operations  13.6 us (2%)
  other arithmetic  7.73 us (1%)
    all_gather x1, waiting for transfers between devices, local(): lax.all_gather(gate_weight, 'fs', axis=0, tiled=True)  128 us
    all_gather x1, waiting for transfers between devices, local(): lax.all_gather(down_weight, 'fs', axis=1, tiled=True)  125 us
    all_gather x1, waiting for transfers between devices, local(): lax.all_gather(up_weight, 'fs', axis=0, tiled=True)  114 us
    ppermute x7, waiting for transfers between devices, gather_around(): parts.append(lax.ppermute(parts[-1], axis, right))  114 us
    all_gather x1, waiting for transfers between devices, local(): lax.all_gather(outer_gate_weight, 'fs', axis=0, tiled=True)  56 us
    all_gather x1, waiting for transfers between devices, local(): lax.all_gather(inner_gate_weight, 'fs', axis=0, tiled=True)  22.4 us
    dot_general x1, matrix products, local(): jnp.dot(picked, down_full, preferred_element_type=jnp.float32)  17.4 us
  transfers between devices with their start and end apart: 17, of which 16 were waited for; matrix products, arithmetic and copies ran while one was open for 5% of the time, Pallas kernels for 0%

profile of v1, /device:TPU:0, one launch (start us, length us, event | category | flops | bytes accessed | tf_op | source)
XLA Modules:
  0.0 688.6 jit_solution(9808848247303414814)
XLA Ops:
  6.5 0.7 all-gather.13.cloned.1.call-update
  7.3 0.0 all-gather.11.cloned.1.call-start
  7.3 0.7 all-gather.11.cloned.1.call-update
  8.1 0.7 all-gather.9.cloned.1.call-update
  8.8 3.0 collective-permute-start
  11.8 12.5 %collective-permute-done = bf16[768,256]{1,0:T(8,128)(2,1)S(1)} collective-permute-done((bf16[768,256]{1,0:T(8,128)(2,1)}, bf16[768,256]{1,0:T(8,128)(2,1)S(1)}, u32[]{:S(2)}, u32[]{:S(2)}) %collective-permute-start) | collective-permute-done | bytes 393248 | tf_op jit(solution)/shard_map/ppermute | solution.py:21
  24.3 2.1 fusion
  26.4 20.4 %collective-permute-done.1 = bf16[768,256]{1,0:T(8,128)(2,1)S(1)} collective-permute-done((bf16[768,256]{1,0:T(8,128)(2,1)S(1)}, bf16[768,256]{1,0:T(8,128)(2,1)S(1)}, u32[]{:S(2)}, u32[]{:S(2)}) %collective-permute-start.1) | collective-permute-done | bytes 393248 | tf_op jit(solution)/shard_map/ppermute | solution.py:21
  46.8 19.6 %collective-permute-done.2 = bf16[768,256]{1,0:T(8,128)(2,1)S(1)} collective-permute-done((bf16[768,256]{1,0:T(8,128)(2,1)S(1)}, bf16[768,256]{1,0:T(8,128)(2,1)S(1)}, u32[]{:S(2)}, u32[]{:S(2)}) %collective-permute-start.2) | collective-permute-done | bytes 393248 | tf_op jit(solution)/shard_map/ppermute | solution.py:21
  66.5 0.8 bitcast_dynamic-update-slice_fusion.7
  67.3 20.4 %collective-permute-done.3 = bf16[768,256]{1,0:T(8,128)(2,1)S(1)} collective-permute-done((bf16[768,256]{1,0:T(8,128)(2,1)S(1)}, bf16[768,256]{1,0:T(8,128)(2,1)S(1)}, u32[]{:S(2)}, u32[]{:S(2)}) %collective-permute-start.3) | collective-permute-done | bytes 393248 | tf_op jit(solution)/shard_map/ppermute | solution.py:21
  87.7 0.8 bitcast_dynamic-update-slice_fusion.6
  88.5 0.8 bitcast_dynamic-update-slice_fusion.5
  89.3 12.0 %collective-permute-done.4 = bf16[768,256]{1,0:T(8,128)(2,1)S(1)} collective-permute-done((bf16[768,256]{1,0:T(8,128)(2,1)S(1)}, bf16[768,256]{1,0:T(8,128)(2,1)S(1)}, u32[]{:S(2)}, u32[]{:S(2)}) %collective-permute-start.4) | collective-permute-done | bytes 393248 | tf_op jit(solution)/shard_map/ppermute | solution.py:21
  101.2 0.8 bitcast_dynamic-update-slice_fusion.4
  102.0 0.8 bitcast_dynamic-update-slice_fusion.3
  102.8 10.0 %collective-permute-done.5 = bf16[768,256]{1,0:T(8,128)(2,1)S(1)} collective-permute-done((bf16[768,256]{1,0:T(8,128)(2,1)S(1)}, bf16[768,256]{1,0:T(8,128)(2,1)S(1)}, u32[]{:S(2)}, u32[]{:S(2)}) %collective-permute-start.5) | collective-permute-done | bytes 393248 | tf_op jit(solution)/shard_map/ppermute | solution.py:21
  112.8 0.8 bitcast_dynamic-update-slice_fusion.2
  113.6 0.8 bitcast_dynamic-update-slice_fusion.1
  114.4 18.8 %collective-permute-done.6 = bf16[768,256]{1,0:T(8,128)(2,1)S(1)} collective-permute-done((bf16[768,256]{1,0:T(8,128)(2,1)S(1)}, bf16[768,256]{1,0:T(8,128)(2,1)S(1)}, u32[]{:S(2)}, u32[]{:S(2)}) %collective-permute-start.6) | collective-permute-done | bytes 393248 | tf_op jit(solution)/shard_map/ppermute | solution.py:21
  133.1 0.8 bitcast_dynamic-update-slice_fusion
  133.9 2.6 gather_fusion
  136.5 2.8 copy.12
  139.3 4.5 convolution_convert_fusion.2
  143.9 22.4 %all-gather.11.cloned.1.call-done = bf16[2048,768]{1,0:T(8,128)(2,1)} async-done(((bf16[256,768]{1,0:T(8,128)(2,1)}), bf16[2048,768]{1,0:T(8,128)(2,1)}) %all-gather.11.cloned.1.call-update) | async-done | bytes 3145744 | tf_op jit(solution)/shard_map/all_gather | solution.py:70
  166.3 4.9 convert_multiply_fusion.4
  171.2 56.0 %all-gather.9.cloned.1.call-done = bf16[2048,768]{1,0:T(8,128)(2,1)} async-done(((bf16[256,768]{1,0:T(8,128)(2,1)}), bf16[2048,768]{1,0:T(8,128)(2,1)}) %all-gather.9.cloned.1.call-update) | async-done | bytes 3145744 | tf_op jit(solution)/shard_map/all_gather | solution.py:69
  227.2 9.9 %convolution_convert_fusion.1 = bf16[512,2048]{1,0:T(8,128)(2,1)} fusion(bf16[768,2048]{0,1:T(8,128)(2,1)} %bitcast.41, f32[512,768]{1,0:T(8,128)} %convert_multiply_fusion.4, f32[511,768]{1,0:T(8,128)} %bitcast.42, f32[510,768]{1,0:T(8,128)} %bitcast.43, bf16[2048,768]{1,0:T(8,128)(2,1)} %all-gather.9.cloned.1.call-done, f32[768]{0:T(1024)S(1)} %get-tuple-element.6, ...), kind=kOutput, calls=%fused_computation.11 | convolution fusion | flops 3230793728 | bytes 15215616 | tf_op jit(solution)/shard_map/dot_general | solution.py:88
  237.2 0.0 all-gather.15.cloned.1.call-start
  237.2 8.5 %reduce-scatter.3.cloned.1.call-done = bf16[256,2048]{1,0:T(8,128)(2,1)} async-done(((bf16[512,2048]{1,0:T(8,128)(2,1)}), bf16[256,2048]{1,0:T(8,128)(2,1)}) %reduce-scatter.3.cloned.1.call-update) | async-done | bytes 1048592 | tf_op jit(solution)/shard_map/reduce_scatter | solution.py:87
  245.7 1.7 fusion.3
  247.5 1.3 fusion.5
  248.8 0.0 all-gather.17.cloned.1.call-start
  248.8 0.5 all-gather.17.cloned.1.call-update
  249.4 0.7 all-gather.19.cloned.1.call-update
  250.2 0.7 all-gather.21.cloned.1.call-update
  250.9 0.2 reduce-scatter.5.cloned.1.call-start
  251.1 9.7 %all-gather.15.cloned.1.call-done = bf16[512,2048]{1,0:T(8,128)(2,1)} async-done(((bf16[256,2048]{1,0:T(8,128)(2,1)}), bf16[512,2048]{1,0:T(8,128)(2,1)}) %all-gather.15.cloned.1.call-update) | async-done | bytes 2097168 | tf_op jit(solution)/shard_map/all_gather | solution.py:95
  260.8 127.7 %all-gather.17.cloned.1.call-done = bf16[2048,2048]{1,0:T(8,128)(2,1)} async-done(((bf16[256,2048]{1,0:T(8,128)(2,1)}), bf16[2048,2048]{1,0:T(8,128)(2,1)}) %all-gather.17.cloned.1.call-update) | async-done | bytes 8388624 | tf_op jit(solution)/shard_map/all_gather | solution.py:72
  388.5 10.5 %fusion.19 = f32[512,2048]{1,0:T(8,128)} fusion(bf16[512,2048]{1,0:T(8,128)(2,1)} %all-gather.15.cloned.1.call-done, bf16[2048,2048]{1,0:T(8,128)(2,1)} %all-gather.17.cloned.1.call-done), kind=kOutput, calls=%fused_computation.50 | convolution fusion | flops 4294967296 | bytes 14680064 | tf_op jit(solution)/shard_map/dot_general | solution.py:96
  399.0 114.3 %all-gather.19.cloned.1.call-done = bf16[2048,2048]{1,0:T(8,128)(2,1)} async-done(((bf16[256,2048]{1,0:T(8,128)(2,1)}), bf16[2048,2048]{1,0:T(8,128)(2,1)}) %all-gather.19.cloned.1.call-update) | async-done | bytes 8388624 | tf_op jit(solution)/shard_map/all_gather | solution.py:73
  513.3 125.2 %all-gather.21.cloned.1.call-done = bf16[2048,2048]{1,0:T(8,128)(2,1)} async-done(((bf16[2048,256]{1,0:T(8,128)(2,1)}), bf16[2048,2048]{1,0:T(8,128)(2,1)}) %all-gather.21.cloned.1.call-update) | async-done | bytes 8388624 | tf_op jit(solution)/shard_map/all_gather | solution.py:74
  638.5 17.4 %convolution_convert_fusion = bf16[512,2048]{1,0:T(8,128)(2,1)} fusion(bf16[2048,2048]{1,0:T(8,128)(2,1)} %all-gather.21.cloned.1.call-done, f32[512,2048]{1,0:T(8,128)} %fusion.19, bf16[512,2048]{1,0:T(8,128)(2,1)S(1)} %copy-done.5, bf16[2048,2048]{1,0:T(8,128)(2,1)} %all-gather.19.cloned.1.call-done), kind=kOutput, calls=%fused_computation.10 | convolution fusion | flops 8597274624 | bytes 25165824 | tf_op jit(solution)/shard_map/dot_general | solution.py:101
  655.9 0.0 all-gather.23.cloned.1.call-start
  656.0 8.0 %reduce-scatter.5.cloned.1.call-done = bf16[256,2048]{1,0:T(8,128)(2,1)} async-done(((bf16[512,2048]{1,0:T(8,128)(2,1)}), bf16[256,2048]{1,0:T(8,128)(2,1)}) %reduce-scatter.5.cloned.1.call-update) | async-done | bytes 1048592 | tf_op jit(solution)/shard_map/reduce_scatter | solution.py:100
  664.0 2.6 fusion.6
  666.6 12.0 %all-gather.23.cloned.1.call-done = bf16[512,2048]{1,0:T(8,128)(2,1)} async-done(((bf16[256,2048]{1,0:T(8,128)(2,1)}), bf16[512,2048]{1,0:T(8,128)(2,1)}) %all-gather.23.cloned.1.call-update) | async-done | bytes 2097168 | tf_op jit(solution)/shard_map/all_gather | solution.py:107
  678.6 3.2 copy.21
  (37 shorter events, 0.3 us)
Async XLA Ops:
  6.5 59.9 %copy-start.1 = (bf16[768,256]{1,0:T(8,128)(2,1)S(1)}, bf16[768,256]{1,0:T(8,128)(2,1)}, u32[]{:S(2)}) copy-start(bf16[768,256]{1,0:T(8,128)(2,1)} %param.17) | copy-start | bytes 1179652
  6.5 59.9 %copy-start.3 = (bf16[2048]{0:T(1024)(128)(2,1)S(1)}, bf16[2048]{0:T(1024)(128)(2,1)}, u32[]{:S(2)}) copy-start(bf16[2048]{0:T(1024)(128)(2,1)} %param.12) | copy-start | bytes 12292
  6.5 59.9 %copy-start.2 = (bf16[3,768]{1,0:T(4,128)(2,1)S(1)}, bf16[3,768]{1,0:T(4,128)(2,1)}, u32[]{:S(2)}) copy-start(bf16[3,768]{1,0:T(4,128)(2,1)} %param.16) | copy-start | bytes 13828
  6.5 132.8 %all-gather.13.cloned.1.call-start = ((), (), s32[]{:S(2)}) async-start(), calls=%async_computation.4 | async-start | bytes 3538944 | tf_op jit(solution)/shard_map/all_gather | solution.py:68
  7.3 159.0 %all-gather.11.cloned.1.call-start = ((), (), s32[]{:S(2)}) async-start(), calls=%async_computation.3 | async-start | bytes 3538944 | tf_op jit(solution)/shard_map/all_gather | solution.py:70
  8.0 219.2 %all-gather.9.cloned.1.call-start = ((), (), s32[]{:S(2)}) async-start(), calls=%async_computation.2 | async-start | bytes 3538944 | tf_op jit(solution)/shard_map/all_gather | solution.py:69
  8.7 237.0 %reduce-scatter.3.cloned.1.call-start = ((), (), s32[]{:S(2)}) async-start(), calls=%async_computation.5 | async-start | bytes 3145728 | tf_op jit(solution)/shard_map/reduce_scatter | solution.py:87
  8.8 15.5 %collective-permute-start = (bf16[768,256]{1,0:T(8,128)(2,1)}, bf16[768,256]{1,0:T(8,128)(2,1)S(1)}, u32[]{:S(2)}, u32[]{:S(2)}) collective-permute-start(bf16[768,256]{1,0:T(8,128)(2,1)} %param.17), channel_id=1, source_target_pairs={{0,2},{2,4},{4,6},{6,8},{8,10},{10,12},{12,14},{14,0},{1,3},{3,5},... | collective-permute-start | bytes 1179656 | tf_op jit(solution)/shard_map/ppermute | solution.py:21
  24.3 22.5 %collective-permute-start.1 = (bf16[768,256]{1,0:T(8,128)(2,1)S(1)}, bf16[768,256]{1,0:T(8,128)(2,1)S(1)}, u32[]{:S(2)}, u32[]{:S(2)}) collective-permute-start(bf16[768,256]{1,0:T(8,128)(2,1)S(1)} %collective-permute-done), channel_id=1, source_target_pairs={{0,2},{2,4},{4,6},{6,8},{8,10},{10,12},{12,14},{14,0},{1,3},{3,5},... | collective-permute-start | bytes 1179656 | tf_op jit(solution)/shard_map/ppermute | solution.py:21
  46.8 19.6 %collective-permute-start.2 = (bf16[768,256]{1,0:T(8,128)(2,1)S(1)}, bf16[768,256]{1,0:T(8,128)(2,1)S(1)}, u32[]{:S(2)}, u32[]{:S(2)}) collective-permute-start(bf16[768,256]{1,0:T(8,128)(2,1)S(1)} %collective-permute-done.1), channel_id=1, source_target_pairs={{0,2},{2,4},{4,6},{6,8},{8,10},{10,12},{12,14},{14,0},{1,3},{3,5},... | collective-permute-start | bytes 1179656 | tf_op jit(solution)/shard_map/ppermute | solution.py:21
  66.4 21.3 %collective-permute-start.3 = (bf16[768,256]{1,0:T(8,128)(2,1)S(1)}, bf16[768,256]{1,0:T(8,128)(2,1)S(1)}, u32[]{:S(2)}, u32[]{:S(2)}) collective-permute-start(bf16[768,256]{1,0:T(8,128)(2,1)S(1)} %collective-permute-done.2), channel_id=1, source_target_pairs={{0,2},{2,4},{4,6},{6,8},{8,10},{10,12},{12,14},{14,0},{1,3},{3,5},... | collective-permute-start | bytes 1179656 | tf_op jit(solution)/shard_map/ppermute | solution.py:21
  87.7 13.5 %collective-permute-start.4 = (bf16[768,256]{1,0:T(8,128)(2,1)S(1)}, bf16[768,256]{1,0:T(8,128)(2,1)S(1)}, u32[]{:S(2)}, u32[]{:S(2)}) collective-permute-start(bf16[768,256]{1,0:T(8,128)(2,1)S(1)} %collective-permute-done.3), channel_id=1, source_target_pairs={{0,2},{2,4},{4,6},{6,8},{8,10},{10,12},{12,14},{14,0},{1,3},{3,5},... | collective-permute-start | bytes 1179656 | tf_op jit(solution)/shard_map/ppermute | solution.py:21
  101.2 11.6 %collective-permute-start.5 = (bf16[768,256]{1,0:T(8,128)(2,1)S(1)}, bf16[768,256]{1,0:T(8,128)(2,1)S(1)}, u32[]{:S(2)}, u32[]{:S(2)}) collective-permute-start(bf16[768,256]{1,0:T(8,128)(2,1)S(1)} %collective-permute-done.4), channel_id=1, source_target_pairs={{0,2},{2,4},{4,6},{6,8},{8,10},{10,12},{12,14},{14,0},{1,3},{3,5},... | collective-permute-start | bytes 1179656 | tf_op jit(solution)/shard_map/ppermute | solution.py:21
  112.8 20.3 %collective-permute-start.6 = (bf16[768,256]{1,0:T(8,128)(2,1)S(1)}, bf16[768,256]{1,0:T(8,128)(2,1)S(1)}, u32[]{:S(2)}, u32[]{:S(2)}) collective-permute-start(bf16[768,256]{1,0:T(8,128)(2,1)S(1)} %collective-permute-done.5), channel_id=1, source_target_pairs={{0,2},{2,4},{4,6},{6,8},{8,10},{10,12},{12,14},{14,0},{1,3},{3,5},... | collective-permute-start | bytes 1179656 | tf_op jit(solution)/shard_map/ppermute | solution.py:21
  139.3 27.0 %copy-start = (bf16[512,2048]{1,0:T(8,128)(2,1)S(1)}, bf16[512,2048]{1,0:T(8,128)(2,1)}, u32[]{:S(2)}) copy-start(bf16[512,2048]{1,0:T(8,128)(2,1)} %param.11) | copy-start | bytes 6291460
  227.2 10.0 %copy-start.4 = (bf16[2048]{0:T(1024)(128)(2,1)S(1)}, bf16[2048]{0:T(1024)(128)(2,1)}, u32[]{:S(2)}) copy-start(bf16[2048]{0:T(1024)(128)(2,1)} %param.18) | copy-start | bytes 12292
  237.2 23.6 %all-gather.15.cloned.1.call-start = ((), (), s32[]{:S(2)}) async-start(), calls=%async_computation.6 | async-start | bytes 3145728 | tf_op jit(solution)/shard_map/all_gather | solution.py:95
  248.8 139.7 %all-gather.17.cloned.1.call-start = ((), (), s32[]{:S(2)}) async-start(), calls=%async_computation.7 | async-start | bytes 9437184 | tf_op jit(solution)/shard_map/all_gather | solution.py:72
  249.4 263.9 %all-gather.19.cloned.1.call-start = ((), (), s32[]{:S(2)}) async-start(), calls=%async_computation.8 | async-start | bytes 9437184 | tf_op jit(solution)/shard_map/all_gather | solution.py:73
  250.1 388.3 %all-gather.21.cloned.1.call-start = ((), (), s32[]{:S(2)}) async-start(), calls=%async_computation.9 | async-start | bytes 9437184 | tf_op jit(solution)/shard_map/all_gather | solution.py:74
  250.9 413.1 %reduce-scatter.5.cloned.1.call-start = ((), (), s32[]{:S(2)}) async-start(), calls=%async_computation.10 | async-start | bytes 3145728 | tf_op jit(solution)/shard_map/reduce_scatter | solution.py:100
  260.8 377.7 %copy-start.5 = (bf16[512,2048]{1,0:T(8,128)(2,1)S(1)}, bf16[512,2048]{1,0:T(8,128)(2,1)}, u32[]{:S(2)}) copy-start(bf16[512,2048]{1,0:T(8,128)(2,1)} %all-gather.15.cloned.1.call-done) | copy-start | bytes 6291460
  655.9 22.7 %all-gather.23.cloned.1.call-start = ((), (), s32[]{:S(2)}) async-start(), calls=%async_computation.11 | async-start | bytes 3145728 | tf_op jit(solution)/shard_map/all_gather | solution.py:107
Sparse Core Ops, SparseCore 0:
  9.5 82.8 all-gather.12
  94.6 71.6 all-gather.10
  168.5 58.6 all-gather.8
  237.3 8.4 reduce-scatter.2
  248.9 11.8 all-gather.14
  262.8 125.6 all-gather.16
  390.6 122.6 all-gather.18
  515.3 123.1 all-gather.20
  656.0 7.8 reduce-scatter.4
  666.7 11.8 all-gather.22
